TPU v7x, 32 devices: a whole 2x2x4 slice. The times are simulated.
32 devices in a mesh: ep: 8 (over z, y), tp: 4 (over x, core).
Axes of the slice: x: 2, y: 2, z: 4, core: 2. Of those that a mesh axis runs over, the one named last changes fastest.
Arguments:
- mixer_in: bfloat16 [4096, 4096], P(('ep', 'tp')), may hold values from -6 to 6
- mixer_gain: float32 [4096], replicated, may hold values from 0.1 to 1.9
- group_weight: bfloat16 [4, 1024, 1024], P('tp'), may hold values from -0.1875 to 0.1875
- group_scale: float32 [4, 1024], P('tp'), may hold values from 0.1 to 1.9
- expert_in: bfloat16 [4096, 4096], P(('ep', 'tp')), may hold values from -6 to 6
- expert_gain: float32 [4096], replicated, may hold values from 0.1 to 1.9
- routes: int32 [4096, 2], P('ep'), may hold values from 0 to 7, all different within a row; in each aligned block of 128 rows (0 to 127, 128 to 255, ...) at most 48 rows name the same one
- route_weight: float32 [4096, 2], P('ep'), may hold values from 0.2 to 1
- gate_weight: bfloat16 [8, 4096, 1024], P('ep', None, 'tp'), may hold values from -0.25 to 0.25
- up_weight: bfloat16 [8, 4096, 1024], P('ep', None, 'tp'), may hold values from -0.25 to 0.25
- down_weight: bfloat16 [8, 1024, 4096], P('ep', 'tp'), may hold values from -0.02734375 to 0.02734375
Outputs:
- mixed: bfloat16 [4096, 4096], P('ep', 'tp')
- expert_out: bfloat16 [4096, 4096], P(('ep', 'tp'))
Inputs may be any that keep to these rules, and one draw needn't show every extreme that they name: `routes`: each row names 2 different experts; within the rows of one device (aligned blocks of 128 rows) no expert is named more than 48 times, and that count is reached.
All inputs are finite; a program needn't handle non-finite values.
Results may differ from a plain program's by a relative error of at most 0.012.
Values may be sent and summed in bfloat16 or wider, within the bound.
A program may use at most 128 MiB of HBM per device.

v0:
```python
import jax
import jax.numpy as jnp
from jax import lax
from jax.sharding import PartitionSpec as P

WMAX = 16
CHUNKS = 3
epsilon = 1e-06
clamp_limit = 7.0
sigmoid_slope = 1.702


def from_behind(x, axis, by):
    count = lax.axis_size(axis)
    pairs = [(i, i + by) for i in range(count) if 0 <= i + by < count]
    return lax.ppermute(x, axis, pairs)


def rms_norm(values, gain):
    widened = values.astype(jnp.float32)
    scaled = widened * lax.rsqrt(jnp.mean(widened * widened, axis=-1, keepdims=True) + epsilon)
    return (scaled * gain).astype(jnp.bfloat16)


def clamped_unit(gate_part, up_part):
    gate_part = jnp.minimum(gate_part, clamp_limit)
    up_part = jnp.clip(up_part, -clamp_limit, clamp_limit)
    return ((up_part + 1.0) * gate_part * jax.nn.sigmoid(sigmoid_slope * gate_part)).astype(
        jnp.bfloat16
    )


def slot_ids(block_routes, experts, capacity):
    onehot = (
        block_routes[:, :, None] == jnp.arange(experts, dtype=jnp.int32)[None, None, :]
    ).astype(jnp.float32)
    per_token = jnp.sum(onehot, axis=1)
    count = block_routes.shape[0]
    before = (
        jnp.arange(count, dtype=jnp.int32)[:, None] > jnp.arange(count, dtype=jnp.int32)[None, :]
    ).astype(jnp.bfloat16)
    earlier = jnp.dot(before, per_token.astype(jnp.bfloat16), preferred_element_type=jnp.float32)
    rank = jnp.sum(onehot * earlier[:, None, :], axis=2).astype(jnp.int32)
    return (block_routes, rank)


def mixer_rows(mixer_in, mixer_gain):
    normed = rms_norm(mixer_in, mixer_gain)
    shard_rows = lax.all_to_all(normed, "tp", split_axis=1, concat_axis=0, tiled=True)
    length = shard_rows.shape[0]
    return (shard_rows, from_behind(shard_rows[length - WMAX :], "ep", 1))


def mixer(shard_rows, before, group_weight, group_scale):
    length = shard_rows.shape[0]
    total = jnp.concatenate([before, shard_rows], axis=0).astype(jnp.float32)
    values = total[WMAX:]
    tp_index = lax.axis_index("tp")
    window = 2 << tp_index
    position = lax.axis_index("ep") * length + jnp.arange(length, dtype=jnp.int32)
    picked = jnp.zeros_like(values)
    reach = 1
    for level in range(lax.axis_size("tp")):
        total = total[reach:] + total[:-reach]
        reach = 2 * reach
        picked = jnp.where(tp_index == level, total[total.shape[0] - length :], picked)
    counts = jnp.minimum(position + 1, window).astype(jnp.float32)[:, None]
    pooled = (picked / counts - values).astype(jnp.bfloat16)
    return (
        jnp.dot(pooled, group_weight[0], preferred_element_type=jnp.float32) * group_scale[0]
    ).astype(jnp.bfloat16)


def shards(
    mixer_in,
    mixer_gain,
    group_weight,
    group_scale,
    expert_in,
    expert_gain,
    routes,
    route_weight,
    gate_weight,
    up_weight,
    down_weight,
):
    shard_rows, before = mixer_rows(mixer_in, mixer_gain)
    expert_in, shard_rows, before = lax.optimization_barrier((expert_in, shard_rows, before))
    mixed = mixer(shard_rows, before, group_weight, group_scale)
    expert_norm = rms_norm(expert_in, expert_gain)
    tok_count, width = expert_in.shape
    top = routes.shape[1]
    experts = lax.axis_size("ep")
    capacity = max(2, 3 * tok_count * top // (2 * experts))
    chunks = CHUNKS if capacity % CHUNKS == 0 else 1
    part = capacity // chunks
    tp_index = lax.axis_index("tp")
    own_routes = lax.dynamic_slice_in_dim(routes, tp_index * tok_count, tok_count, 0)
    own_weight = lax.dynamic_slice_in_dim(route_weight, tp_index * tok_count, tok_count, 0)
    gate_local = gate_weight[0]
    up_local = up_weight[0]
    down_full = lax.all_gather(down_weight[0], "tp", axis=0, tiled=True)
    expert_of, rank = slot_ids(own_routes, experts, capacity)
    expert_sum = jnp.zeros((tok_count, width), jnp.float32)
    pieces = []
    picks = []
    for chunk in range(chunks):
        inside = (rank >= chunk * part) & (rank < (chunk + 1) * part)
        slot = jnp.where(inside, expert_of * part + rank - chunk * part, -1)
        match = slot[:, :, None] == jnp.arange(experts * part, dtype=jnp.int32)[None, None, :]
        picks.append(match)
        pick = jnp.any(match, axis=1).astype(jnp.bfloat16)
        outgoing = lax.dot_general(
            pick, expert_norm, (((0,), (0,)), ((), ())), preferred_element_type=jnp.float32
        ).astype(jnp.bfloat16)
        if chunk > 0:
            outgoing, arrived = lax.optimization_barrier((outgoing, arrived))
        arrived = lax.all_to_all(outgoing, "ep", split_axis=0, concat_axis=0, tiled=True)
        if chunk == 1:
            arrived, down_full = lax.optimization_barrier((arrived, down_full))
        pieces.append(lax.all_gather(arrived, "tp", axis=0, tiled=True))
    for chunk in range(chunks):
        piece = pieces[chunk]
        if chunk > 0:
            piece, result = lax.optimization_barrier((piece, result))
        hidden = clamped_unit(
            jnp.dot(piece, gate_local, preferred_element_type=jnp.float32),
            jnp.dot(piece, up_local, preferred_element_type=jnp.float32),
        )
        hidden = lax.all_to_all(hidden, "tp", split_axis=0, concat_axis=1, tiled=True)
        result = jnp.dot(hidden, down_full, preferred_element_type=jnp.float32).astype(jnp.bfloat16)
        returned = lax.all_to_all(result, "ep", split_axis=0, concat_axis=0, tiled=True)
        weights = jnp.sum(jnp.where(picks[chunk], own_weight[:, :, None], 0.0), axis=1)
        high = weights.astype(jnp.bfloat16)
        low = (weights - high.astype(jnp.float32)).astype(jnp.bfloat16)
        expert_sum = (
            expert_sum
            + jnp.dot(high, returned, preferred_element_type=jnp.float32)
            + jnp.dot(low, returned, preferred_element_type=jnp.float32)
        )
    return (mixed, expert_sum.astype(jnp.bfloat16))


def solution(mesh):
    in_specs = (
        P(("ep", "tp"), None),
        P(),
        P("tp", None, None),
        P("tp", None),
        P(("ep", "tp"), None),
        P(),
        P("ep", None),
        P("ep", None),
        P("ep", None, "tp"),
        P("ep", None, "tp"),
        P("ep", "tp", None),
    )
    out_specs = (P("ep", "tp"), P(("ep", "tp"), None))
    return jax.shard_map(shards, mesh=mesh, in_specs=in_specs, out_specs=out_specs, check_vma=False)
```

profile of v0, /device:TPU:0, one launch (start us, length us, event | category | flops | bytes accessed | tf_op | source)
XLA Modules:
  0.0 288.4 jit_solution(611450616829126164)
XLA Ops:
  11.6 4.4 %all-to-all-start = ((bf16[128,4,1024]{0,2,1:T(8,128)(2,1)}), bf16[128,4,1024]{0,2,1:T(8,128)(2,1)}, u32[]{:S(2)}, u32[]{:S(2)}) async-start(bf16[128,4,1024]{0,2,1:T(8,128)(2,1)} %bitcast.115), calls=%async_computation | async-start | bytes 2097152 | tf_op jit(solution)/shard_map/all_to_all | solution.py:49
  16.3 22.9 %all-to-all-done = bf16[128,4,1024]{0,2,1:T(8,128)(2,1)} async-done(((bf16[128,4,1024]{0,2,1:T(8,128)(2,1)}), bf16[128,4,1024]{0,2,1:T(8,128)(2,1)}, u32[]{:S(2)}, u32[]{:S(2)}) %all-to-all-start) | async-done | bytes 1048608 | tf_op jit(solution)/shard_map/all_to_all | solution.py:49
  42.3 5.4 %collective-permute-start = (bf16[16,1024]{1,0:T(8,128)(2,1)S(1)}, bf16[16,1024]{1,0:T(8,128)(2,1)}, u32[]{:S(2)}, u32[]{:S(2)}) collective-permute-start(bf16[16,1024]{1,0:T(8,128)(2,1)S(1)} %slice.56), channel_id=1, source_target_pairs={{0,4},{4,8},{8,12},{12,16},{16,20},{20,24},{24,28},{1,5},{5,9},{9,... | collective-permute-start | bytes 98312 | tf_op jit(solution)/shard_map/ppermute | solution.py:16
  49.4 30.4 %all_to_all.148 = bf16[8,16,4096]{2,1,0:T(8,128)(2,1)} all-to-all(bf16[8,16,4096]{2,1,0:T(8,128)(2,1)S(1)} %bitcast.117), channel_id=1, replica_groups=mesh['ep'=8,'tp'=4] {'ep'}, dimensions={0} | all-to-all | bytes 2097152 | tf_op jit(solution)/shard_map/all_to_all | solution.py:118
  80.5 28.0 %all_to_all.149 = bf16[8,16,4096]{2,1,0:T(8,128)(2,1)} all-to-all(bf16[8,16,4096]{2,1,0:T(8,128)(2,1)S(1)} %bitcast.118), channel_id=1, replica_groups=mesh['ep'=8,'tp'=4] {'ep'}, dimensions={0} | all-to-all | bytes 2097152 | tf_op jit(solution)/shard_map/all_to_all | solution.py:118
  109.1 28.9 %all_to_all.150 = bf16[8,16,4096]{2,1,0:T(8,128)(2,1)} all-to-all(bf16[8,16,4096]{2,1,0:T(8,128)(2,1)S(1)} %bitcast.116), channel_id=1, replica_groups=mesh['ep'=8,'tp'=4] {'ep'}, dimensions={0} | all-to-all | bytes 2097152 | tf_op jit(solution)/shard_map/all_to_all | solution.py:118
  138.1 4.3 %fusion.28 = f32[512,256]{1,0:T(8,128)S(1)} fusion(bf16[512,4096]{1,0:T(8,128)(2,1)} %all-gather.6.cloned.1.call-done, bf16[1,4096,256]{2,1,0:T(8,128)(2,1)} %param.19), kind=kOutput, calls=%fused_computation.48 | convolution fusion | flops 1073872896 | bytes 6815744 | tf_op jit(solution)/shard_map/dot_general | solution.py:127
  144.3 8.8 %all_to_all.151 = bf16[4,128,256]{1,2,0:T(8,128)(2,1)S(1)} all-to-all(bf16[4,128,256]{1,2,0:T(8,128)(2,1)S(1)} %copy.41), channel_id=1, replica_groups=mesh['ep'=8,'tp'=4] {'tp'}, dimensions={0} | all-to-all | bytes 524288 | tf_op jit(solution)/shard_map/all_to_all | solution.py:130
  153.2 5.6 %convolution_convert_fusion.3 = bf16[128,4096]{1,0:T(8,128)(2,1)} fusion(bf16[128,1024]{0,1:T(8,128)(2,1)S(1)} %bitcast.127, bf16[1024,4096]{1,0:T(8,128)(2,1)} %bitcast.106), kind=kOutput, calls=%fused_computation.9 | convolution fusion | flops 1074266112 | bytes 9699328 | tf_op jit(solution)/shard_map/dot_general | solution.py:131
  158.8 4.9 %fusion.31 = f32[512,256]{1,0:T(8,128)S(1)} fusion(bf16[512,4096]{1,0:T(8,128)(2,1)} %all-gather.8.cloned.1.call-done, bf16[1,4096,256]{2,1,0:T(8,128)(2,1)} %param.19), kind=kOutput, calls=%fused_computation.49 | convolution fusion | flops 1073872896 | bytes 6815744 | tf_op jit(solution)/shard_map/dot_general | solution.py:127
  166.4 11.6 %all_to_all.152 = bf16[4,128,256]{1,2,0:T(8,128)(2,1)S(1)} all-to-all(bf16[4,128,256]{1,2,0:T(8,128)(2,1)S(1)} %copy.42), channel_id=1, replica_groups=mesh['ep'=8,'tp'=4] {'tp'}, dimensions={0} | all-to-all | bytes 524288 | tf_op jit(solution)/shard_map/all_to_all | solution.py:130
  178.0 4.0 %all-to-all-start.4 = ((bf16[8,16,4096]{2,1,0:T(8,128)(2,1)}), bf16[8,16,4096]{2,1,0:T(8,128)(2,1)S(1)}, u32[]{:S(2)}, u32[]{:S(2)}) async-start(bf16[8,16,4096]{2,1,0:T(8,128)(2,1)} %bitcast.123), calls=%async_computation.4 | async-start | bytes 2097152 | tf_op jit(solution)/shard_map/all_to_all | solution.py:132
  183.5 5.7 %convolution_convert_fusion.2 = bf16[128,4096]{1,0:T(8,128)(2,1)} fusion(bf16[128,1024]{0,1:T(8,128)(2,1)S(1)} %bitcast.126, bf16[1024,4096]{1,0:T(8,128)(2,1)} %bitcast.107), kind=kOutput, calls=%fused_computation.8 | convolution fusion | flops 1074266112 | bytes 9699328 | tf_op jit(solution)/shard_map/dot_general | solution.py:131
  191.1 4.3 %fusion.34 = f32[512,256]{1,0:T(8,128)S(1)} fusion(bf16[512,4096]{1,0:T(8,128)(2,1)} %all-gather.10.cloned.1.call-done, bf16[1,4096,256]{2,1,0:T(8,128)(2,1)} %param.19), kind=kOutput, calls=%fused_computation.50 | convolution fusion | flops 1073872896 | bytes 6815744 | tf_op jit(solution)/shard_map/dot_general | solution.py:127
  197.9 9.8 %all-to-all-done.4 = bf16[8,16,4096]{2,1,0:T(8,128)(2,1)S(1)} async-done(((bf16[8,16,4096]{2,1,0:T(8,128)(2,1)}), bf16[8,16,4096]{2,1,0:T(8,128)(2,1)S(1)}, u32[]{:S(2)}, u32[]{:S(2)}) %all-to-all-start.4) | async-done | bytes 1048608 | tf_op jit(solution)/shard_map/all_to_all | solution.py:132
  207.7 3.4 %all-to-all-start.8 = ((bf16[4,128,256]{1,2,0:T(8,128)(2,1)}), bf16[4,128,256]{1,2,0:T(8,128)(2,1)S(1)}, u32[]{:S(2)}, u32[]{:S(2)}) async-start(bf16[4,128,256]{1,2,0:T(8,128)(2,1)} %copy.43), calls=%async_computation.8 | async-start | bytes 524288 | tf_op jit(solution)/shard_map/all_to_all | solution.py:130
  211.2 2.9 %maximum_convert_fusion = f32[528,1024]{1,0:T(8,128)} fusion(bf16[512,1024]{1,0:T(8,128)(2,1)} %bitcast.114, bf16[16,1024]{1,0:T(8,128)(2,1)} %collective-permute-done), kind=kLoop, calls=%fused_computation.66 | loop fusion | flops 2162688 | bytes 3244032 | tf_op jit(solution)/shard_map/convert_element_type | solution.py:56
  214.1 3.0 %all-to-all-done.8 = bf16[4,128,256]{1,2,0:T(8,128)(2,1)S(1)} async-done(((bf16[4,128,256]{1,2,0:T(8,128)(2,1)}), bf16[4,128,256]{1,2,0:T(8,128)(2,1)S(1)}, u32[]{:S(2)}, u32[]{:S(2)}) %all-to-all-start.8) | async-done | bytes 262176 | tf_op jit(solution)/shard_map/all_to_all | solution.py:130
  217.1 4.2 %all-to-all-start.6 = ((bf16[8,16,4096]{2,1,0:T(8,128)(2,1)}), bf16[8,16,4096]{2,1,0:T(8,128)(2,1)}, u32[]{:S(2)}, u32[]{:S(2)}) async-start(bf16[8,16,4096]{2,1,0:T(8,128)(2,1)} %bitcast.122), calls=%async_computation.6 | async-start | bytes 2097152 | tf_op jit(solution)/shard_map/all_to_all | solution.py:132
  233.6 13.5 %all-to-all-done.6 = bf16[8,16,4096]{2,1,0:T(8,128)(2,1)} async-done(((bf16[8,16,4096]{2,1,0:T(8,128)(2,1)}), bf16[8,16,4096]{2,1,0:T(8,128)(2,1)}, u32[]{:S(2)}, u32[]{:S(2)}) %all-to-all-start.6) | async-done | bytes 1048608 | tf_op jit(solution)/shard_map/all_to_all | solution.py:132
  247.1 4.2 %all-to-all-start.9 = ((bf16[8,16,4096]{2,1,0:T(8,128)(2,1)}), bf16[8,16,4096]{2,1,0:T(8,128)(2,1)}, u32[]{:S(2)}, u32[]{:S(2)}) async-start(bf16[8,16,4096]{2,1,0:T(8,128)(2,1)} %bitcast.124), calls=%async_computation.9 | async-start | bytes 2097152 | tf_op jit(solution)/shard_map/all_to_all | solution.py:132
  251.4 7.7 %multiply_convert_fusion = bf16[512,1024]{1,0:T(8,128)(2,1)} fusion(bf16[1,1024,1024]{2,1,0:T(8,128)(2,1)S(1)} %copy-done, f32[1024]{0:T(1024)S(1)} %bitcast.131, f32[528,1024]{1,0:T(8,128)} %maximum_convert_fusion, f32[527,1024]{1,0:T(8,128)} %copy-done.1, f32[525,1024]{1,0:T(8,128)} %copy-done.2, f32[521,1024]{1,0:T(8,128)} %copy-done.3, ...), kind=kOutput, calls=%fused_computation.47 | convolution fusion | flops 1078984704 | bytes 15734788 | tf_op jit(solution)/shard_map/dot_general | solution.py:70
  261.9 3.0 %convolution_add_fusion.2 = f32[128,4096]{1,0:T(8,128)} fusion(f32[128,4096]{1,0:T(8,128)S(1)} %convolution_add_fusion.3, bf16[128,4096]{1,0:T(8,128)(2,1)} %bitcast.21, f32[128,128]{1,0:T(8,128)S(1)} %copy-done.5), kind=kOutput, calls=%fused_computation.2 | convolution fusion | flops 134807552 | bytes 5308416 | tf_op jit(solution)/shard_map/dot_general | solution.py:139
  264.9 12.0 %all-to-all-done.9 = bf16[8,16,4096]{2,1,0:T(8,128)(2,1)} async-done(((bf16[8,16,4096]{2,1,0:T(8,128)(2,1)}), bf16[8,16,4096]{2,1,0:T(8,128)(2,1)}, u32[]{:S(2)}, u32[]{:S(2)}) %all-to-all-start.9) | async-done | bytes 1048608 | tf_op jit(solution)/shard_map/all_to_all | solution.py:132
  (87 shorter events, 41.4 us)
Async XLA Ops:
  7.2 244.2 %copy-start = (bf16[1,1024,1024]{2,1,0:T(8,128)(2,1)S(1)}, bf16[1,1024,1024]{2,1,0:T(8,128)(2,1)}, u32[]{:S(2)}) copy-start(bf16[1,1024,1024]{2,1,0:T(8,128)(2,1)} %param.13) | copy-start | bytes 6291460
  7.2 101.4 %all-gather.12.cloned.1.call-start = ((), (), s32[]{:S(2)}) async-start(), calls=%async_computation.13 | async-start | bytes 10485760 | tf_op jit(solution)/shard_map/all_gather | solution.py:102
  10.1 6.0 %copy-start.8 = (s32[512,2]{0,1:T(2,128)S(1)}, s32[512,2]{0,1:T(2,128)}, u32[]{:S(2)}) copy-start(s32[512,2]{0,1:T(2,128)} %param.17) | copy-start | bytes 12292
  11.6 37.0 %copy-start.4 = (bf16[128,4096]{1,0:T(8,128)(2,1)S(1)}, bf16[128,4096]{1,0:T(8,128)(2,1)}, u32[]{:S(2)}) copy-start(bf16[128,4096]{1,0:T(8,128)(2,1)} %param.15) | copy-start | bytes 3145732
  11.6 27.6 %all-to-all-start = ((bf16[128,4,1024]{0,2,1:T(8,128)(2,1)}), bf16[128,4,1024]{0,2,1:T(8,128)(2,1)}, u32[]{:S(2)}, u32[]{:S(2)}) async-start(bf16[128,4,1024]{0,2,1:T(8,128)(2,1)} %bitcast.115), calls=%async_computation | async-start | bytes 2097152 | tf_op jit(solution)/shard_map/all_to_all | solution.py:49
  16.0 32.9 %copy-start.6 = (f32[4096]{0:T(1024)S(1)}, f32[4096]{0:T(1024)}, u32[]{:S(2)}) copy-start(f32[4096]{0:T(1024)} %param.16) | copy-start | bytes 49156
  16.0 122.0 %all-gather.6.cloned.1.call-start = ((), (), s32[]{:S(2)}) async-start(), calls=%async_computation.10 | async-start | bytes 5242880 | tf_op jit(solution)/shard_map/all_gather | solution.py:121
  42.3 6.3 %collective-permute-start = (bf16[16,1024]{1,0:T(8,128)(2,1)S(1)}, bf16[16,1024]{1,0:T(8,128)(2,1)}, u32[]{:S(2)}, u32[]{:S(2)}) collective-permute-start(bf16[16,1024]{1,0:T(8,128)(2,1)S(1)} %slice.56), channel_id=1, source_target_pairs={{0,4},{4,8},{8,12},{12,16},{16,20},{20,24},{24,28},{1,5},{5,9},{9,... | collective-permute-start | bytes 98312 | tf_op jit(solution)/shard_map/ppermute | solution.py:16
  79.9 79.0 %all-gather.8.cloned.1.call-start = ((), (), s32[]{:S(2)}) async-start(), calls=%async_computation.11 | async-start | bytes 5242880 | tf_op jit(solution)/shard_map/all_gather | solution.py:121
  108.6 82.5 %all-gather.10.cloned.1.call-start = ((), (), s32[]{:S(2)}) async-start(), calls=%async_computation.12 | async-start | bytes 5242880 | tf_op jit(solution)/shard_map/all_gather | solution.py:121
  138.1 4.3 %copy-start.10 = (bf16[512,4096]{1,0:T(8,128)(2,1)S(1)}, bf16[512,4096]{1,0:T(8,128)(2,1)}, u32[]{:S(2)}) copy-start(bf16[512,4096]{1,0:T(8,128)(2,1)} %all-gather.6.cloned.1.call-done) | copy-start | bytes 12582916
  138.1 4.8 %copy-start.12 = (bf16[1,4096,256]{2,1,0:T(8,128)(2,1)S(1)}, bf16[1,4096,256]{2,1,0:T(8,128)(2,1)}, u32[]{:S(2)}) copy-start(bf16[1,4096,256]{2,1,0:T(8,128)(2,1)} %param.20) | copy-start | bytes 6291460
  158.8 5.4 %copy-start.11 = (bf16[512,4096]{1,0:T(8,128)(2,1)S(1)}, bf16[512,4096]{1,0:T(8,128)(2,1)}, u32[]{:S(2)}) copy-start(bf16[512,4096]{1,0:T(8,128)(2,1)} %all-gather.8.cloned.1.call-done) | copy-start | bytes 12582916
  158.8 6.1 %copy-start.13 = (bf16[1,4096,256]{2,1,0:T(8,128)(2,1)S(1)}, bf16[1,4096,256]{2,1,0:T(8,128)(2,1)}, u32[]{:S(2)}) copy-start(bf16[1,4096,256]{2,1,0:T(8,128)(2,1)} %param.20) | copy-start | bytes 6291460
  178.0 29.7 %all-to-all-start.4 = ((bf16[8,16,4096]{2,1,0:T(8,128)(2,1)}), bf16[8,16,4096]{2,1,0:T(8,128)(2,1)S(1)}, u32[]{:S(2)}, u32[]{:S(2)}) async-start(bf16[8,16,4096]{2,1,0:T(8,128)(2,1)} %bitcast.123), calls=%async_computation.4 | async-start | bytes 2097152 | tf_op jit(solution)/shard_map/all_to_all | solution.py:132
  191.1 4.3 %copy-start.9 = (bf16[512,4096]{1,0:T(8,128)(2,1)S(1)}, bf16[512,4096]{1,0:T(8,128)(2,1)}, u32[]{:S(2)}) copy-start(bf16[512,4096]{1,0:T(8,128)(2,1)} %all-gather.10.cloned.1.call-done) | copy-start | bytes 12582916
  191.1 4.7 %copy-start.14 = (bf16[1,4096,256]{2,1,0:T(8,128)(2,1)S(1)}, bf16[1,4096,256]{2,1,0:T(8,128)(2,1)}, u32[]{:S(2)}) copy-start(bf16[1,4096,256]{2,1,0:T(8,128)(2,1)} %param.20) | copy-start | bytes 6291460
  207.7 9.4 %all-to-all-start.8 = ((bf16[4,128,256]{1,2,0:T(8,128)(2,1)}), bf16[4,128,256]{1,2,0:T(8,128)(2,1)S(1)}, u32[]{:S(2)}, u32[]{:S(2)}) async-start(bf16[4,128,256]{1,2,0:T(8,128)(2,1)} %copy.43), calls=%async_computation.8 | async-start | bytes 524288 | tf_op jit(solution)/shard_map/all_to_all | solution.py:130
  217.1 30.0 %all-to-all-start.6 = ((bf16[8,16,4096]{2,1,0:T(8,128)(2,1)}), bf16[8,16,4096]{2,1,0:T(8,128)(2,1)}, u32[]{:S(2)}, u32[]{:S(2)}) async-start(bf16[8,16,4096]{2,1,0:T(8,128)(2,1)} %bitcast.122), calls=%async_computation.6 | async-start | bytes 2097152 | tf_op jit(solution)/shard_map/all_to_all | solution.py:132
  224.1 5.9 %slice-start = ((s8[8388608]{0:T(1024)(128)(4,1)}), s8[4194304]{0:T(1024)(128)(4,1)S(1)}, s32[]{:S(2)}) async-start(s8[8388608]{0:T(1024)(128)(4,1)} %bitcast.108), calls=%async_computation.14 | async-start | bytes 8388608
  225.5 5.9 %slice-start.1 = ((s8[8388608]{0:T(1024)(128)(4,1)}), s8[4194304]{0:T(1024)(128)(4,1)S(1)}, s32[]{:S(2)}) async-start(s8[8388608]{0:T(1024)(128)(4,1)} %bitcast.108), calls=%async_computation.15 | async-start | bytes 8388608
  226.8 3.2 %copy-start.3 = (f32[521,1024]{1,0:T(8,128)}, f32[521,1024]{1,0:T(8,128)S(1)}, u32[]{:S(2)}) copy-start(f32[521,1024]{1,0:T(8,128)S(1)} %slice_add_fusion) | copy-start | bytes 6402052
  233.6 17.7 %copy-start.15 = (f32[1,1024]{1,0:T(1,128)S(1)}, f32[1,1024]{1,0:T(1,128)}, u32[]{:S(2)}) copy-start(f32[1,1024]{1,0:T(1,128)} %param.14) | copy-start | bytes 12292
  247.1 29.8 %all-to-all-start.9 = ((bf16[8,16,4096]{2,1,0:T(8,128)(2,1)}), bf16[8,16,4096]{2,1,0:T(8,128)(2,1)}, u32[]{:S(2)}, u32[]{:S(2)}) async-start(bf16[8,16,4096]{2,1,0:T(8,128)(2,1)} %bitcast.124), calls=%async_computation.9 | async-start | bytes 2097152 | tf_op jit(solution)/shard_map/all_to_all | solution.py:132
  (4 other events, 5.7 us)
Sparse Core Ops, SparseCore 0:
  9.5 68.2 all-gather.11
  80.0 34.9 all-gather.5
  116.5 34.4 all-gather.7
  152.4 38.6 all-gather.9
where the time goes:
time: 289 us; the launch traced here: 288 us
  blocking collectives  108 us (37%)
  waiting for transfers between devices  64.7 us (22%)
  matrix products  50.6 us (18%)
  starting transfers between devices  25.8 us (9%)
  local copies, waits for them, and re-layouts  15.6 us (5%)
  between operations  14.1 us (5%)
  other arithmetic  9.82 us (3%)
    all_to_all x3, blocking collectives, shards(): lax.all_to_all(outgoing, 'ep', split_axis=0, concat_axis=0, tiled=True)  87.3 us
    all_to_all x3, waiting for transfers between devices, shards(): lax.all_to_all(result, 'ep', split_axis=0, concat_axis=0, tiled=True)  35.2 us
    all_to_all x1, waiting for transfers between devices, mixer_rows(): lax.all_to_all(normed, 'tp', split_axis=1, concat_axis=0, tiled=True)  22.9 us
    all_to_all x2, blocking collectives, shards(): lax.all_to_all(hidden, 'tp', split_axis=0, concat_axis=1, tiled=True)  20.5 us
    dot_general x3, matrix products, shards(): jnp.dot(hidden, down_full, preferred_element_type=jnp.float32)  13.6 us
    dot_general x3, matrix products, shards(): jnp.dot(piece, gate_local, preferred_element_type=jnp.float32)  13.4 us
    all_to_all x3, starting transfers between devices, shards(): lax.all_to_all(result, 'ep', split_axis=0, concat_axis=0, tiled=True)  12.5 us
    unnamed x37, local copies, waits for them, and re-layouts  8.1 us
  transfers between devices with their start and end apart: 10, of which 7 were waited for; matrix products, arithmetic and copies ran while one was open for 22% of the time, Pallas kernels for 0%

commit v1 on v0

--- a/solution.py
+++ b/solution.py
@@ -127,7 +127,10 @@
             jnp.dot(piece, gate_local, preferred_element_type=jnp.float32),
             jnp.dot(piece, up_local, preferred_element_type=jnp.float32),
         )
-        hidden = lax.all_to_all(hidden, "tp", split_axis=0, concat_axis=1, tiled=True)
+        hidden = jnp.concatenate(
+            lax.all_to_all(jnp.stack(jnp.split(hidden, lax.axis_size("tp"), axis=0)), "tp", 0, 0),
+            axis=1,
+        )
         result = jnp.dot(hidden, down_full, preferred_element_type=jnp.float32).astype(jnp.bfloat16)
         returned = lax.all_to_all(result, "ep", split_axis=0, concat_axis=0, tiled=True)
         weights = jnp.sum(jnp.where(picks[chunk], own_weight[:, :, None], 0.0), axis=1)

time: 289 us -> 292 us (1.010)
  blocking collectives: 108 us -> 87.3 us
  waiting for transfers between devices: 64.7 us -> 75.6 us
  starting transfers between devices: 25.8 us -> 32.8 us
  matrix products: 50.6 us -> 54 us
    all_to_all x2 -> x0, blocking collectives: 20.5 us -> none  [shards(): lax.all_to_all(hidden, 'tp', split_axis=0, concat_axis=1, tiled=True)]
    all_to_all x1 -> x3, waiting for transfers between devices: 3.04 us -> 16.7 us  [shards(): lax.all_to_all(jnp.stack(jnp.split(hidden, lax.axis_size('tp'), axis=0)),...]
    all_to_all x1 -> x3, starting transfers between devices: 3.4 us -> 10.2 us  [shards(): lax.all_to_all(jnp.stack(jnp.split(hidden, lax.axis_size('tp'), axis=0)),...]
    dot_general x3, matrix products: 13.6 us -> 17 us  [shards(): jnp.dot(hidden, down_full, preferred_element_type=jnp.float32)]
  transfers between devices with their start and end apart: 10 -> 12, of which waited for: 7 -> 8; matrix products, arithmetic and copies ran while one was open for 22% -> 25% of each run, Pallas kernels for 0% -> 0%
where the time goes in v1:
time: 292 us; the launch traced here: 291 us
  blocking collectives  87.3 us (30%)
  waiting for transfers between devices  75.6 us (26%)
  matrix products  54 us (18%)
  starting transfers between devices  32.8 us (11%)
  local copies, waits for them, and re-layouts  14.7 us (5%)
  between operations  14.2 us (5%)
  other arithmetic  12.3 us (4%)
    all_to_all x3, blocking collectives, shards(): lax.all_to_all(outgoing, 'ep', split_axis=0, concat_axis=0, tiled=True)  87.3 us
    all_to_all x3, waiting for transfers between devices, shards(): lax.all_to_all(result, 'ep', split_axis=0, concat_axis=0, tiled=True)  34.4 us
    all_to_all x1, waiting for transfers between devices, mixer_rows(): lax.all_to_all(normed, 'tp', split_axis=1, concat_axis=0, tiled=True)  22.9 us
    dot_general x3, matrix products, shards(): jnp.dot(hidden, down_full, preferred_element_type=jnp.float32)  17 us
    all_to_all x3, waiting for transfers between devices, shards(): lax.all_to_all(jnp.stack(jnp.split(hidden, lax.axis_size('tp'), axis=0)),...  16.7 us
    dot_general x3, matrix products, shards(): jnp.dot(piece, gate_local, preferred_element_type=jnp.float32)  13.4 us
    all_to_all x3, starting transfers between devices, shards(): lax.all_to_all(result, 'ep', split_axis=0, concat_axis=0, tiled=True)  12.6 us
    all_to_all x3, starting transfers between devices, shards(): lax.all_to_all(jnp.stack(jnp.split(hidden, lax.axis_size('tp'), axis=0)),...  10.2 us
  transfers between devices with their start and end apart: 12, of which 8 were waited for; matrix products, arithmetic and copies ran while one was open for 25% of the time, Pallas kernels for 0%

profile of v1, /device:TPU:0, one launch (start us, length us, event | category | flops | bytes accessed | tf_op | source)
XLA Modules:
  0.0 290.8 jit_solution(7579406890513456842)
XLA Ops:
  11.6 4.4 %all-to-all-start = ((bf16[128,4,1024]{0,2,1:T(8,128)(2,1)}), bf16[128,4,1024]{0,2,1:T(8,128)(2,1)}, u32[]{:S(2)}, u32[]{:S(2)}) async-start(bf16[128,4,1024]{0,2,1:T(8,128)(2,1)} %bitcast.131), calls=%async_computation | async-start | bytes 2097152 | tf_op jit(solution)/shard_map/all_to_all | solution.py:49
  16.3 22.9 %all-to-all-done = bf16[128,4,1024]{0,2,1:T(8,128)(2,1)} async-done(((bf16[128,4,1024]{0,2,1:T(8,128)(2,1)}), bf16[128,4,1024]{0,2,1:T(8,128)(2,1)}, u32[]{:S(2)}, u32[]{:S(2)}) %all-to-all-start) | async-done | bytes 1048608 | tf_op jit(solution)/shard_map/all_to_all | solution.py:49
  42.3 5.4 %collective-permute-start = (bf16[16,1024]{1,0:T(8,128)(2,1)S(1)}, bf16[16,1024]{1,0:T(8,128)(2,1)}, u32[]{:S(2)}, u32[]{:S(2)}) collective-permute-start(bf16[16,1024]{1,0:T(8,128)(2,1)S(1)} %slice.56), channel_id=1, source_target_pairs={{0,4},{4,8},{8,12},{12,16},{16,20},{20,24},{24,28},{1,5},{5,9},{9,... | collective-permute-start | bytes 98312 | tf_op jit(solution)/shard_map/ppermute | solution.py:16
  49.5 30.4 %all_to_all.106 = bf16[8,16,4096]{2,1,0:T(8,128)(2,1)} all-to-all(bf16[8,16,4096]{2,1,0:T(8,128)(2,1)S(1)} %bitcast.133), channel_id=1, replica_groups=mesh['ep'=8,'tp'=4] {'ep'}, dimensions={0} | all-to-all | bytes 2097152 | tf_op jit(solution)/shard_map/all_to_all | solution.py:118
  80.6 28.0 %all_to_all.107 = bf16[8,16,4096]{2,1,0:T(8,128)(2,1)} all-to-all(bf16[8,16,4096]{2,1,0:T(8,128)(2,1)S(1)} %bitcast.134), channel_id=1, replica_groups=mesh['ep'=8,'tp'=4] {'ep'}, dimensions={0} | all-to-all | bytes 2097152 | tf_op jit(solution)/shard_map/all_to_all | solution.py:118
  109.2 28.9 %all_to_all.108 = bf16[8,16,4096]{2,1,0:T(8,128)(2,1)} all-to-all(bf16[8,16,4096]{2,1,0:T(8,128)(2,1)S(1)} %bitcast.132), channel_id=1, replica_groups=mesh['ep'=8,'tp'=4] {'ep'}, dimensions={0} | all-to-all | bytes 2097152 | tf_op jit(solution)/shard_map/all_to_all | solution.py:118
  138.1 4.3 %fusion.28 = f32[512,256]{1,0:T(8,128)S(1)} fusion(bf16[512,4096]{1,0:T(8,128)(2,1)} %all-gather.6.cloned.1.call-done, bf16[1,4096,256]{2,1,0:T(8,128)(2,1)} %param.19), kind=kOutput, calls=%fused_computation.48 | convolution fusion | flops 1073872896 | bytes 6815744 | tf_op jit(solution)/shard_map/dot_general | solution.py:127
  145.0 3.4 %all-to-all-start.2 = ((bf16[4,128,256]{2,1,0:T(8,128)(2,1)}), bf16[4,128,256]{2,1,0:T(8,128)(2,1)S(1)}, u32[]{:S(2)}, u32[]{:S(2)}) async-start(bf16[4,128,256]{2,1,0:T(8,128)(2,1)} %pad_maximum_fusion), calls=%async_computation.2 | async-start | bytes 524288 | tf_op jit(solution)/shard_map/all_to_all | solution.py:131
  148.4 6.0 %all-to-all-done.2 = bf16[4,128,256]{2,1,0:T(8,128)(2,1)S(1)} async-done(((bf16[4,128,256]{2,1,0:T(8,128)(2,1)}), bf16[4,128,256]{2,1,0:T(8,128)(2,1)S(1)}, u32[]{:S(2)}, u32[]{:S(2)}) %all-to-all-start.2) | async-done | bytes 262176 | tf_op jit(solution)/shard_map/all_to_all | solution.py:131
  154.5 5.6 %convolution_convert_fusion.3 = bf16[128,4096]{1,0:T(8,128)(2,1)} fusion(bf16[128,1024]{0,1:T(8,128)(2,1)S(1)} %bitcast.142, bf16[1024,4096]{1,0:T(8,128)(2,1)} %bitcast.124), kind=kOutput, calls=%fused_computation.9 | convolution fusion | flops 1074266112 | bytes 9699328 | tf_op jit(solution)/shard_map/dot_general | solution.py:134
  160.2 4.9 %fusion.31 = f32[512,256]{1,0:T(8,128)S(1)} fusion(bf16[512,4096]{1,0:T(8,128)(2,1)} %all-gather.8.cloned.1.call-done, bf16[1,4096,256]{2,1,0:T(8,128)(2,1)} %param.19), kind=kOutput, calls=%fused_computation.49 | convolution fusion | flops 1073872896 | bytes 6815744 | tf_op jit(solution)/shard_map/dot_general | solution.py:127
  167.6 3.4 %all-to-all-start.5 = ((bf16[4,128,256]{2,1,0:T(8,128)(2,1)}), bf16[4,128,256]{2,1,0:T(8,128)(2,1)S(1)}, u32[]{:S(2)}, u32[]{:S(2)}) async-start(bf16[4,128,256]{2,1,0:T(8,128)(2,1)} %pad_maximum_fusion.1), calls=%async_computation.5 | async-start | bytes 524288 | tf_op jit(solution)/shard_map/all_to_all | solution.py:131
  172.6 7.7 %all-to-all-done.5 = bf16[4,128,256]{2,1,0:T(8,128)(2,1)S(1)} async-done(((bf16[4,128,256]{2,1,0:T(8,128)(2,1)}), bf16[4,128,256]{2,1,0:T(8,128)(2,1)S(1)}, u32[]{:S(2)}, u32[]{:S(2)}) %all-to-all-start.5) | async-done | bytes 262176 | tf_op jit(solution)/shard_map/all_to_all | solution.py:131
  180.3 4.1 %all-to-all-start.4 = ((bf16[8,16,4096]{2,1,0:T(8,128)(2,1)}), bf16[8,16,4096]{2,1,0:T(8,128)(2,1)S(1)}, u32[]{:S(2)}, u32[]{:S(2)}) async-start(bf16[8,16,4096]{2,1,0:T(8,128)(2,1)} %bitcast.138), calls=%async_computation.4 | async-start | bytes 2097152 | tf_op jit(solution)/shard_map/all_to_all | solution.py:135
  185.5 5.7 %convolution_convert_fusion.2 = bf16[128,4096]{1,0:T(8,128)(2,1)} fusion(bf16[128,1024]{0,1:T(8,128)(2,1)S(1)} %bitcast.143, bf16[1024,4096]{1,0:T(8,128)(2,1)} %bitcast.125), kind=kOutput, calls=%fused_computation.8 | convolution fusion | flops 1074266112 | bytes 9699328 | tf_op jit(solution)/shard_map/dot_general | solution.py:134
  191.2 4.3 %fusion.34 = f32[512,256]{1,0:T(8,128)S(1)} fusion(bf16[512,4096]{1,0:T(8,128)(2,1)} %all-gather.10.cloned.1.call-done, bf16[1,4096,256]{2,1,0:T(8,128)(2,1)} %param.19), kind=kOutput, calls=%fused_computation.50 | convolution fusion | flops 1073872896 | bytes 6815744 | tf_op jit(solution)/shard_map/dot_general | solution.py:127
  198.0 12.1 %all-to-all-done.4 = bf16[8,16,4096]{2,1,0:T(8,128)(2,1)S(1)} async-done(((bf16[8,16,4096]{2,1,0:T(8,128)(2,1)}), bf16[8,16,4096]{2,1,0:T(8,128)(2,1)S(1)}, u32[]{:S(2)}, u32[]{:S(2)}) %all-to-all-start.4) | async-done | bytes 1048608 | tf_op jit(solution)/shard_map/all_to_all | solution.py:135
  210.1 3.4 %all-to-all-start.8 = ((bf16[4,128,256]{2,1,0:T(8,128)(2,1)}), bf16[4,128,256]{2,1,0:T(8,128)(2,1)S(1)}, u32[]{:S(2)}, u32[]{:S(2)}) async-start(bf16[4,128,256]{2,1,0:T(8,128)(2,1)} %pad_maximum_fusion.2), calls=%async_computation.8 | async-start | bytes 524288 | tf_op jit(solution)/shard_map/all_to_all | solution.py:131
  219.5 4.2 %all-to-all-start.6 = ((bf16[8,16,4096]{2,1,0:T(8,128)(2,1)}), bf16[8,16,4096]{2,1,0:T(8,128)(2,1)}, u32[]{:S(2)}, u32[]{:S(2)}) async-start(bf16[8,16,4096]{2,1,0:T(8,128)(2,1)} %bitcast.139), calls=%async_computation.6 | async-start | bytes 2097152 | tf_op jit(solution)/shard_map/all_to_all | solution.py:135
  233.6 5.6 %convolution_convert_fusion = bf16[128,4096]{1,0:T(8,128)(2,1)} fusion(bf16[128,1024]{0,1:T(8,128)(2,1)S(1)} %bitcast.141, bf16[1024,4096]{1,0:T(8,128)(2,1)} %bitcast.126), kind=kOutput, calls=%fused_computation.6 | convolution fusion | flops 1074266112 | bytes 9699328 | tf_op jit(solution)/shard_map/dot_general | solution.py:134
  239.2 10.3 %all-to-all-done.6 = bf16[8,16,4096]{2,1,0:T(8,128)(2,1)} async-done(((bf16[8,16,4096]{2,1,0:T(8,128)(2,1)}), bf16[8,16,4096]{2,1,0:T(8,128)(2,1)}, u32[]{:S(2)}, u32[]{:S(2)}) %all-to-all-start.6) | async-done | bytes 1048608 | tf_op jit(solution)/shard_map/all_to_all | solution.py:135
  249.5 4.2 %all-to-all-start.9 = ((bf16[8,16,4096]{2,1,0:T(8,128)(2,1)}), bf16[8,16,4096]{2,1,0:T(8,128)(2,1)}, u32[]{:S(2)}, u32[]{:S(2)}) async-start(bf16[8,16,4096]{2,1,0:T(8,128)(2,1)} %bitcast.140), calls=%async_computation.9 | async-start | bytes 2097152 | tf_op jit(solution)/shard_map/all_to_all | solution.py:135
  253.8 7.7 %multiply_convert_fusion = bf16[512,1024]{1,0:T(8,128)(2,1)} fusion(bf16[1,1024,1024]{2,1,0:T(8,128)(2,1)S(1)} %copy-done, f32[1024]{0:T(1024)S(1)} %bitcast.147, f32[528,1024]{1,0:T(8,128)} %maximum_convert_fusion, f32[527,1024]{1,0:T(8,128)} %copy-done.1, f32[525,1024]{1,0:T(8,128)} %copy-done.2, f32[521,1024]{1,0:T(8,128)} %copy-done.3, ...), kind=kOutput, calls=%fused_computation.47 | convolution fusion | flops 1078984704 | bytes 15734788 | tf_op jit(solution)/shard_map/dot_general | solution.py:70
  267.3 12.0 %all-to-all-done.9 = bf16[8,16,4096]{2,1,0:T(8,128)(2,1)} async-done(((bf16[8,16,4096]{2,1,0:T(8,128)(2,1)}), bf16[8,16,4096]{2,1,0:T(8,128)(2,1)}, u32[]{:S(2)}, u32[]{:S(2)}) %all-to-all-start.9) | async-done | bytes 1048608 | tf_op jit(solution)/shard_map/all_to_all | solution.py:135
  (94 shorter events, 47.7 us)
Async XLA Ops:
  7.2 246.6 %copy-start = (bf16[1,1024,1024]{2,1,0:T(8,128)(2,1)S(1)}, bf16[1,1024,1024]{2,1,0:T(8,128)(2,1)}, u32[]{:S(2)}) copy-start(bf16[1,1024,1024]{2,1,0:T(8,128)(2,1)} %param.13) | copy-start | bytes 6291460
  7.2 101.4 %all-gather.12.cloned.1.call-start = ((), (), s32[]{:S(2)}) async-start(), calls=%async_computation.13 | async-start | bytes 10485760 | tf_op jit(solution)/shard_map/all_gather | solution.py:102
  10.1 6.0 %copy-start.10 = (s32[512,2]{0,1:T(2,128)S(1)}, s32[512,2]{0,1:T(2,128)}, u32[]{:S(2)}) copy-start(s32[512,2]{0,1:T(2,128)} %param.17) | copy-start | bytes 12292
  11.6 37.0 %copy-start.4 = (bf16[128,4096]{1,0:T(8,128)(2,1)S(1)}, bf16[128,4096]{1,0:T(8,128)(2,1)}, u32[]{:S(2)}) copy-start(bf16[128,4096]{1,0:T(8,128)(2,1)} %param.15) | copy-start | bytes 3145732
  11.6 27.6 %all-to-all-start = ((bf16[128,4,1024]{0,2,1:T(8,128)(2,1)}), bf16[128,4,1024]{0,2,1:T(8,128)(2,1)}, u32[]{:S(2)}, u32[]{:S(2)}) async-start(bf16[128,4,1024]{0,2,1:T(8,128)(2,1)} %bitcast.131), calls=%async_computation | async-start | bytes 2097152 | tf_op jit(solution)/shard_map/all_to_all | solution.py:49
  16.0 32.9 %copy-start.8 = (f32[4096]{0:T(1024)S(1)}, f32[4096]{0:T(1024)}, u32[]{:S(2)}) copy-start(f32[4096]{0:T(1024)} %param.16) | copy-start | bytes 49156
  16.0 122.1 %all-gather.6.cloned.1.call-start = ((), (), s32[]{:S(2)}) async-start(), calls=%async_computation.10 | async-start | bytes 5242880 | tf_op jit(solution)/shard_map/all_gather | solution.py:121
  42.3 6.4 %collective-permute-start = (bf16[16,1024]{1,0:T(8,128)(2,1)S(1)}, bf16[16,1024]{1,0:T(8,128)(2,1)}, u32[]{:S(2)}, u32[]{:S(2)}) collective-permute-start(bf16[16,1024]{1,0:T(8,128)(2,1)S(1)} %slice.56), channel_id=1, source_target_pairs={{0,4},{4,8},{8,12},{12,16},{16,20},{20,24},{24,28},{1,5},{5,9},{9,... | collective-permute-start | bytes 98312 | tf_op jit(solution)/shard_map/ppermute | solution.py:16
  79.9 80.3 %all-gather.8.cloned.1.call-start = ((), (), s32[]{:S(2)}) async-start(), calls=%async_computation.11 | async-start | bytes 5242880 | tf_op jit(solution)/shard_map/all_gather | solution.py:121
  108.6 82.6 %all-gather.10.cloned.1.call-start = ((), (), s32[]{:S(2)}) async-start(), calls=%async_computation.12 | async-start | bytes 5242880 | tf_op jit(solution)/shard_map/all_gather | solution.py:121
  138.1 4.3 %copy-start.13 = (bf16[512,4096]{1,0:T(8,128)(2,1)S(1)}, bf16[512,4096]{1,0:T(8,128)(2,1)}, u32[]{:S(2)}) copy-start(bf16[512,4096]{1,0:T(8,128)(2,1)} %all-gather.6.cloned.1.call-done) | copy-start | bytes 12582916
  138.1 4.8 %copy-start.14 = (bf16[1,4096,256]{2,1,0:T(8,128)(2,1)S(1)}, bf16[1,4096,256]{2,1,0:T(8,128)(2,1)}, u32[]{:S(2)}) copy-start(bf16[1,4096,256]{2,1,0:T(8,128)(2,1)} %param.20) | copy-start | bytes 6291460
  145.0 9.4 %all-to-all-start.2 = ((bf16[4,128,256]{2,1,0:T(8,128)(2,1)}), bf16[4,128,256]{2,1,0:T(8,128)(2,1)S(1)}, u32[]{:S(2)}, u32[]{:S(2)}) async-start(bf16[4,128,256]{2,1,0:T(8,128)(2,1)} %pad_maximum_fusion), calls=%async_computation.2 | async-start | bytes 524288 | tf_op jit(solution)/shard_map/all_to_all | solution.py:131
  160.2 4.9 %copy-start.12 = (bf16[512,4096]{1,0:T(8,128)(2,1)S(1)}, bf16[512,4096]{1,0:T(8,128)(2,1)}, u32[]{:S(2)}) copy-start(bf16[512,4096]{1,0:T(8,128)(2,1)} %all-gather.8.cloned.1.call-done) | copy-start | bytes 12582916
  160.2 5.4 %copy-start.15 = (bf16[1,4096,256]{2,1,0:T(8,128)(2,1)S(1)}, bf16[1,4096,256]{2,1,0:T(8,128)(2,1)}, u32[]{:S(2)}) copy-start(bf16[1,4096,256]{2,1,0:T(8,128)(2,1)} %param.20) | copy-start | bytes 6291460
  167.6 12.6 %all-to-all-start.5 = ((bf16[4,128,256]{2,1,0:T(8,128)(2,1)}), bf16[4,128,256]{2,1,0:T(8,128)(2,1)S(1)}, u32[]{:S(2)}, u32[]{:S(2)}) async-start(bf16[4,128,256]{2,1,0:T(8,128)(2,1)} %pad_maximum_fusion.1), calls=%async_computation.5 | async-start | bytes 524288 | tf_op jit(solution)/shard_map/all_to_all | solution.py:131
  180.3 29.8 %all-to-all-start.4 = ((bf16[8,16,4096]{2,1,0:T(8,128)(2,1)}), bf16[8,16,4096]{2,1,0:T(8,128)(2,1)S(1)}, u32[]{:S(2)}, u32[]{:S(2)}) async-start(bf16[8,16,4096]{2,1,0:T(8,128)(2,1)} %bitcast.138), calls=%async_computation.4 | async-start | bytes 2097152 | tf_op jit(solution)/shard_map/all_to_all | solution.py:135
  191.2 4.3 %copy-start.11 = (bf16[512,4096]{1,0:T(8,128)(2,1)S(1)}, bf16[512,4096]{1,0:T(8,128)(2,1)}, u32[]{:S(2)}) copy-start(bf16[512,4096]{1,0:T(8,128)(2,1)} %all-gather.10.cloned.1.call-done) | copy-start | bytes 12582916
  191.2 4.7 %copy-start.16 = (bf16[1,4096,256]{2,1,0:T(8,128)(2,1)S(1)}, bf16[1,4096,256]{2,1,0:T(8,128)(2,1)}, u32[]{:S(2)}) copy-start(bf16[1,4096,256]{2,1,0:T(8,128)(2,1)} %param.20) | copy-start | bytes 6291460
  210.1 9.4 %all-to-all-start.8 = ((bf16[4,128,256]{2,1,0:T(8,128)(2,1)}), bf16[4,128,256]{2,1,0:T(8,128)(2,1)S(1)}, u32[]{:S(2)}, u32[]{:S(2)}) async-start(bf16[4,128,256]{2,1,0:T(8,128)(2,1)} %pad_maximum_fusion.2), calls=%async_computation.8 | async-start | bytes 524288 | tf_op jit(solution)/shard_map/all_to_all | solution.py:131
  219.5 7.1 %copy-start.5 = (bf16[4,128,256]{2,1,0:T(8,128)(2,1)}, bf16[4,128,256]{2,1,0:T(8,128)(2,1)S(1)}, u32[]{:S(2)}) copy-start(bf16[4,128,256]{2,1,0:T(8,128)(2,1)S(1)} %all-to-all-done.8) | copy-start | bytes 786436
  219.5 30.0 %all-to-all-start.6 = ((bf16[8,16,4096]{2,1,0:T(8,128)(2,1)}), bf16[8,16,4096]{2,1,0:T(8,128)(2,1)}, u32[]{:S(2)}, u32[]{:S(2)}) async-start(bf16[8,16,4096]{2,1,0:T(8,128)(2,1)} %bitcast.139), calls=%async_computation.6 | async-start | bytes 2097152 | tf_op jit(solution)/shard_map/all_to_all | solution.py:135
  239.2 14.6 %copy-start.17 = (f32[1,1024]{1,0:T(1,128)S(1)}, f32[1,1024]{1,0:T(1,128)}, u32[]{:S(2)}) copy-start(f32[1,1024]{1,0:T(1,128)} %param.14) | copy-start | bytes 12292
  249.5 29.8 %all-to-all-start.9 = ((bf16[8,16,4096]{2,1,0:T(8,128)(2,1)}), bf16[8,16,4096]{2,1,0:T(8,128)(2,1)}, u32[]{:S(2)}, u32[]{:S(2)}) async-start(bf16[8,16,4096]{2,1,0:T(8,128)(2,1)} %bitcast.140), calls=%async_computation.9 | async-start | bytes 2097152 | tf_op jit(solution)/shard_map/all_to_all | solution.py:135
  (6 other events, 12.6 us)
Sparse Core Ops, SparseCore 0:
  9.5 68.1 all-gather.11
  80.0 34.9 all-gather.5
  116.5 34.4 all-gather.7
  152.5 37.2 all-gather.9
